TPU v7x, 32 devices: a whole 2x2x4 slice. The times are simulated.
32 devices in a mesh: ep: 8 (over z, x), tp: 4 (over y, core).
Axes of the slice: x: 2, y: 2, z: 4, core: 2. Of those that a mesh axis runs over, the one named last changes fastest.
Arguments:
- tokens: bfloat16 [64, 1024], P('ep'), may hold values from -6 to 6
- kv_cache: bfloat16 [64, 4, 1024, 128], P('ep', 'tp'), may hold values from -6 to 6
- lengths: int32 [64], P('ep'), may hold values from 256 to 1024
- w_query: bfloat16 [1024, 512], P(None, 'tp'), may hold values from -0.1875 to 0.1875
- w_key: bfloat16 [1024, 256], P(None, 'tp'), may hold values from -0.1875 to 0.1875
- w_value: bfloat16 [1024, 256], P(None, 'tp'), may hold values from -0.1875 to 0.1875
- break_bias: float32 [8], P('tp'), may hold values from -7.5 to -3.5
- head_gain: float32 [512], P('tp'), may hold values from 0.1 to 1.9
- w_output: bfloat16 [512, 1024], P('tp'), may hold values from -0.25 to 0.25
- attn_norm_gain: float32 [1024], replicated, may hold values from 0.1 to 1.9
- w_router: bfloat16 [1024, 16], replicated, may hold values from -0.1875 to 0.1875
- routes: int32 [64, 2], P('ep'), may hold values from 0 to 15, all different within a row; in each aligned block of 8 rows (0 to 7, 8 to 15, ...) at most 2 rows name the same one
- expert_gate: bfloat16 [1024, 57344], P(None, ('ep', 'tp')), may hold values from -0.1875 to 0.1875
- expert_up: bfloat16 [1024, 57344], P(None, ('ep', 'tp')), may hold values from -0.1875 to 0.1875
- expert_down: bfloat16 [57344, 1024], P(('ep', 'tp')), may hold values from -0.09375 to 0.09375
- dense_gate: bfloat16 [1024, 2816], P(None, 'ep'), may hold values from -0.1875 to 0.1875
- dense_up: bfloat16 [1024, 2816], P(None, 'ep'), may hold values from -0.1875 to 0.1875
- dense_down: bfloat16 [2816, 1024], P('ep', 'tp'), may hold values from -0.109375 to 0.109375
- mix_gate: bfloat16 [1024], replicated, may hold values from -0.1875 to 0.1875
- ffn_norm_gain: float32 [1024], P('tp'), may hold values from 0.1 to 1.9
Outputs:
- layer_out: bfloat16 [64, 1024], P('ep', 'tp')
- new_kv: bfloat16 [64, 4, 128], P('ep', 'tp')
Inputs may be any that keep to these rules, and one draw needn't show every extreme that they name: lengths[b] is the number of valid cached positions of sequence b and the new token's position. `routes`: each row names 2 different experts. Among the rows of one index of ep (aligned blocks of 8 rows) no expert is named more than 2 times, a bound that some block reaches.
All inputs are finite; a program needn't handle non-finite values.
Results may differ from a plain program's by a relative error of at most 0.012.
Values may be sent and summed in bfloat16 or wider, within the bound.
A program may use at most 128 MiB of HBM per device.

v0:
```python
import jax
import jax.numpy as jnp
from jax import lax
from jax.sharding import PartitionSpec as P

FE = 3584
CAP = 2


RESIDUAL_SCALE = 8.0**0.25
PRECISE = lax.Precision.HIGHEST


def layer_norm(values, gain):
    centre = jnp.mean(values, axis=-1, keepdims=True)
    centred = values - centre
    spread = jnp.mean(centred * centred, axis=-1, keepdims=True)
    return centred * lax.rsqrt(spread + 1e-05) * gain


def stick_weights(scores, visible):
    survive = jnp.where(visible, jax.nn.log_sigmoid(-scores), 0.0)
    remaining = lax.cumsum(survive, axis=3, reverse=True) - survive
    return jnp.where(visible, jnp.exp(jax.nn.log_sigmoid(scores) + remaining), 0.0)


def body(
    tokens,
    kv_cache,
    lengths,
    w_query,
    w_key,
    w_value,
    break_bias,
    head_gain,
    w_output,
    attn_norm_gain,
    w_router,
    routes,
    expert_gate,
    expert_up,
    expert_down,
    dense_gate,
    dense_up,
    dense_down,
    mix_gate,
    ffn_norm_gain,
):
    seq_count = tokens.shape[0]
    model_width = tokens.shape[1]
    key_heads = kv_cache.shape[1]
    positions = kv_cache.shape[2]
    head_dim = kv_cache.shape[3] // 2
    local_heads = w_query.shape[1] // head_dim
    group_size = local_heads // key_heads
    queries = jnp.dot(tokens, w_query, preferred_element_type=jnp.float32).astype(jnp.bfloat16)
    queries = queries.reshape(seq_count, key_heads, group_size, head_dim)
    key_new = jnp.dot(tokens, w_key, preferred_element_type=jnp.float32).astype(jnp.bfloat16)
    value_new = jnp.dot(tokens, w_value, preferred_element_type=jnp.float32).astype(jnp.bfloat16)
    new_kv = jnp.concatenate(
        [
            key_new.reshape(seq_count, key_heads, head_dim),
            value_new.reshape(seq_count, key_heads, head_dim),
        ],
        axis=2,
    )
    cached_keys = kv_cache[..., :head_dim]
    cached_values = kv_cache[..., head_dim:]
    scores = jnp.einsum(
        "bgqd,bgld->bgql", queries, cached_keys, preferred_element_type=jnp.float32
    ) * head_dim ** (-0.5)
    scores = scores + break_bias.reshape(1, key_heads, group_size, 1)
    visible = lax.broadcasted_iota(jnp.int32, (seq_count, 1, 1, positions), 3) < lengths.reshape(
        seq_count, 1, 1, 1
    )
    weights = stick_weights(scores, visible).astype(jnp.bfloat16)
    blended = jnp.einsum(
        "bgql,bgld->bgqd", weights, cached_values, preferred_element_type=jnp.float32
    )
    rescale = lax.rsqrt(jnp.mean(blended * blended, axis=3, keepdims=True) + 1e-06)
    normed = ((blended * rescale).reshape(seq_count, local_heads * head_dim) * head_gain).astype(
        jnp.bfloat16
    )
    partial_out = jnp.dot(normed, w_output, preferred_element_type=jnp.float32)
    attended = lax.psum(partial_out.astype(jnp.bfloat16), "tp").astype(jnp.float32)
    settled = layer_norm(
        RESIDUAL_SCALE * tokens.astype(jnp.float32) + attended, attn_norm_gain
    ).astype(jnp.bfloat16)
    experts = w_router.shape[1]
    top_count = routes.shape[1]
    logits = jnp.dot(settled, w_router, preferred_element_type=jnp.float32)
    chosen = routes[:, :, None] == lax.broadcasted_iota(
        jnp.int32, (seq_count, top_count, experts), 2
    )
    picked = jnp.sum(jnp.where(chosen, logits[:, None, :], 0.0), axis=2)
    route_weight = jax.nn.sigmoid(picked - picked[:, ::-1])
    assigned = chosen.reshape(seq_count * top_count, experts).astype(jnp.int32)
    before = jnp.cumsum(assigned, axis=0) - assigned
    slot_index = jnp.sum(before * assigned, axis=1)
    slot_hits = (
        slot_index[:, None] == lax.broadcasted_iota(jnp.int32, (seq_count * top_count, CAP), 1)
    ).astype(jnp.int32)
    placement = (assigned[:, :, None] * slot_hits[:, None, :]).reshape(
        seq_count, top_count, experts * CAP
    )
    selector = jnp.sum(placement, axis=1).astype(jnp.bfloat16)
    weighted = jnp.sum(placement.astype(jnp.float32) * route_weight[:, :, None], axis=1)
    buffer = lax.dot_general(
        selector, settled, (((0,), (0,)), ((), ())), preferred_element_type=jnp.float32
    )
    buffer = buffer.astype(jnp.bfloat16).reshape(experts, CAP, model_width)
    hosts = lax.axis_size("ep")
    tp_size = lax.axis_size("tp")
    if experts >= hosts:
        per_host = experts // hosts
        outgoing = buffer.reshape(hosts, per_host, CAP, model_width)
    else:
        per_host = 1
        outgoing = jnp.repeat(buffer, hosts // experts, axis=0).reshape(hosts, 1, CAP, model_width)
    columns = expert_gate.shape[1]
    block_index = lax.axis_index(("ep", "tp"))
    own_expert = block_index * columns // FE
    local_slot = own_expert - lax.axis_index("ep") * experts // hosts
    slice_width = model_width // tp_size
    arrived = lax.all_to_all(outgoing, "ep", split_axis=0, concat_axis=0, tiled=True)
    slot_count = arrived.shape[2]
    received = lax.dynamic_index_in_dim(arrived, local_slot, 1, keepdims=False)
    received = received.reshape(hosts * slot_count, model_width)
    gate_pre = jnp.dot(received, expert_gate, preferred_element_type=jnp.float32)
    up_pre = jnp.dot(received, expert_up, preferred_element_type=jnp.float32)
    hidden = (jax.nn.silu(gate_pre) * up_pre).astype(jnp.bfloat16)
    partial_value = jnp.dot(hidden, expert_down, preferred_element_type=jnp.float32)
    partial_value = partial_value.reshape(hosts, 1, slot_count, model_width)
    slot_mask = (lax.broadcasted_iota(jnp.int32, (1, per_host, 1, 1), 1) == local_slot).astype(
        jnp.float32
    )
    summed = lax.psum_scatter(
        (partial_value * slot_mask).astype(jnp.bfloat16), "tp", scatter_dimension=3, tiled=True
    ).astype(jnp.float32)
    returned = lax.all_to_all(
        summed.astype(jnp.bfloat16), "ep", split_axis=0, concat_axis=0, tiled=True
    ).astype(summed.dtype)
    host_ids = lax.broadcasted_iota(jnp.int32, (hosts * per_host,), 0)
    host_expert = host_ids // per_host * experts // hosts + host_ids % per_host
    ownership = (
        host_expert[None, :] == lax.broadcasted_iota(jnp.int32, (experts, hosts * per_host), 0)
    ).astype(jnp.float32)
    gathered = jnp.dot(
        ownership, returned.reshape(hosts * per_host, CAP * slice_width), precision=PRECISE
    )
    gathered = gathered.reshape(experts * CAP, slice_width)
    routed = jnp.dot(weighted, gathered, precision=PRECISE)
    column_rank = lax.axis_index("tp")
    own_settled = lax.dynamic_slice_in_dim(settled, column_rank * slice_width, slice_width, 1)
    shard_rows = lax.all_gather(settled, "ep", axis=0, tiled=True)
    gate_pre = jnp.dot(shard_rows, dense_gate, preferred_element_type=jnp.float32)
    up_pre = jnp.dot(shard_rows, dense_up, preferred_element_type=jnp.float32)
    dense_hidden = (jax.nn.silu(gate_pre) * up_pre).astype(jnp.bfloat16)
    own_hidden = lax.all_to_all(dense_hidden, "ep", split_axis=0, concat_axis=1, tiled=True)
    dense_out = jnp.dot(
        own_hidden,
        lax.all_gather(dense_down, "ep", axis=0, tiled=True),
        preferred_element_type=jnp.float32,
    )
    mix_weight = jax.nn.sigmoid(jnp.dot(settled, mix_gate, preferred_element_type=jnp.float32))
    combined = (
        RESIDUAL_SCALE * own_settled.astype(jnp.float32) + routed + mix_weight[:, None] * dense_out
    )
    row_sums, squares = lax.psum(
        (jnp.sum(combined, axis=1), jnp.sum(combined * combined, axis=1)), "tp"
    )
    row_mean = row_sums / model_width
    row_var = squares / model_width - row_mean * row_mean
    result = (
        (combined - row_mean[:, None]) * lax.rsqrt(row_var[:, None] + 1e-05) * ffn_norm_gain
    ).astype(jnp.bfloat16)
    return (result, new_kv)


def solution(mesh):
    in_specs = (
        P("ep", None),
        P("ep", "tp", None, None),
        P("ep"),
        P(None, "tp"),
        P(None, "tp"),
        P(None, "tp"),
        P("tp"),
        P("tp"),
        P("tp", None),
        P(),
        P(),
        P("ep", None),
        P(None, ("ep", "tp")),
        P(None, ("ep", "tp")),
        P(("ep", "tp"), None),
        P(None, "ep"),
        P(None, "ep"),
        P("ep", "tp"),
        P(),
        P("tp"),
    )
    out_specs = (P("ep", "tp"), P("ep", "tp", None))
    return jax.shard_map(body, mesh=mesh, in_specs=in_specs, out_specs=out_specs, check_vma=False)
```

profile of v0, /device:TPU:0, one launch (start us, length us, event | category | flops | bytes accessed | tf_op | source)
XLA Modules:
  0.0 162.0 jit_solution(14771551961724182834)
XLA Ops:
  8.0 0.9 copy.50
  9.1 0.2 select_reduce_fusion.1
  9.6 0.7 iota_compare_fusion
  10.3 1.1 convolution_convert_fusion.4
  11.6 2.3 %fusion.32 = (f32[8,2,1024]{2,1,0:T(2,128)S(1)}, f32[8,2,1024]{2,1,0:T(2,128)S(1)}) fusion(pred[8,1024]{1,0:T(8,128)(4,1)S(1)} %iota_compare_fusion, f32[2]{0:T(128)} %param.26, bf16[8,2,64]{2,1,0:T(2,128)(2,1)S(1)} %reshape.259, bf16[8,1,1024,128]{3,2,1,0:T(8,128)(2,1)} %param.21), kind=kOutput, calls=%fused_computation.41 | convolution fusion | flops 2260992 | bytes 2238472 | tf_op jit(solution)/shard_map/bgqd,bgld->bgql/dot_general | solution.py:69
  13.9 19.8 %reduce-window.6 = f32[8,1,2,8,128]{4,3,2,1,0:T(8,128)S(1)} reduce-window(f32[8,1,2,8,128]{4,3,2,1,0:T(8,128)S(1)} %bitcast.77, f32[]{:T(128)} %constant.97.clone.1), window={size=1x1x1x1x128 pad=0_0x0_0x0_0x0_0x0_127}, to_apply=%region_0.1 | reduce-window | flops 2080768 | bytes 131076 | tf_op jit(solution)/shard_map/reduce-window
  33.8 0.2 copy.47
  34.0 0.3 reduce-window.9
  34.5 1.1 multiply_reduce_fusion.3
  36.0 12.7 %psum.21 = bf16[8,1024]{1,0:T(8,128)(2,1)S(1)} all-reduce(bf16[8,1024]{1,0:T(8,128)(2,1)S(1)} %convolution_convert_fusion.1), channel_id=1, replica_groups=mesh['ep'=8,'tp'=4] {'tp'}, use_global_device_ids=true, to_apply=%region_3.4 | all-reduce | flops 8192 | bytes 32768 | tf_op jit(solution)/shard_map/psum | solution.py:85
  48.8 0.2 multiply_reduce_fusion
  49.1 0.2 convolution_convert_fusion
  49.3 0.7 reshape_reshape.3
  50.0 5.8 %all-to-all-start = ((bf16[8,2,2,1024]{3,2,1,0:T(2,128)(2,1)}), bf16[8,2,2,1024]{3,2,1,0:T(2,128)(2,1)S(1)}, u32[]{:S(2)}, u32[]{:S(2)}) async-start(bf16[8,2,2,1024]{3,2,1,0:T(2,128)(2,1)} %reshape_reshape.3), calls=%async_computation | async-start | bytes 131072 | tf_op jit(solution)/shard_map/all_to_all | solution.py:125
  55.9 6.8 %all-to-all-done = bf16[8,2,2,1024]{3,2,1,0:T(2,128)(2,1)S(1)} async-done(((bf16[8,2,2,1024]{3,2,1,0:T(2,128)(2,1)}), bf16[8,2,2,1024]{3,2,1,0:T(2,128)(2,1)S(1)}, u32[]{:S(2)}, u32[]{:S(2)}) %all-to-all-start) | async-done | bytes 65568 | tf_op jit(solution)/shard_map/all_to_all | solution.py:125
  62.8 2.6 %fusion.49 = f32[16,1792]{1,0:T(8,128)S(1)} fusion(bf16[16,1024]{1,0:T(8,128)(2,1)S(1)} %reshape.268, bf16[1024,1792]{1,0:T(8,128)(2,1)} %param.32), kind=kOutput, calls=%fused_computation.94 | convolution fusion | flops 58720256 | bytes 3817472 | tf_op jit(solution)/shard_map/dot_general | solution.py:129
  65.4 4.2 %fusion.14 = f32[16,1024]{1,0:T(8,128)S(1)} fusion(bf16[1792,1024]{1,0:T(8,128)(2,1)} %param.34, bf16[16,1024]{1,0:T(8,128)(2,1)S(1)} %reshape.268, bf16[1024,1792]{1,0:T(8,128)(2,1)} %param.33, f32[16,1792]{1,0:T(8,128)S(1)} %fusion.49), kind=kOutput, calls=%fused_computation.13 | convolution fusion | flops 117612544 | bytes 7553024 | tf_op jit(solution)/shard_map/dot_general | solution.py:132
  69.8 7.8 %copy.53 = bf16[8,2,2,1024]{2,1,0,3:T(2,128)(2,1)} copy(bf16[8,2,2,1024]{3,2,1,0:T(2,128)(2,1)S(1)} %multiply_convert_fusion) | data formatting | bytes 131072
  77.6 12.3 %reshape.275 = bf16[1024,32]{1,0:T(8,128)(2,1)} reshape(bf16[1024,8,2,2]{3,2,1,0:T(2,128)(2,1)} %bitcast.74) | data formatting | bytes 131072
  89.9 0.5 all-gather.2.cloned.1.call-update
  90.5 30.9 %all_gather.6 = bf16[64,1024]{1,0:T(8,128)(2,1)S(1)} all-gather(bf16[8,1024]{1,0:T(8,128)(2,1)S(1)} %multiply_convert_fusion.1), channel_id=1, replica_groups=mesh['ep'=8,'tp'=4] {'ep'}, dimensions={0}, use_global_device_ids=true | all-gather | bytes 147456 | tf_op jit(solution)/shard_map/all_gather | solution.py:155
  121.4 0.3 fusion.50
  121.8 1.0 fusion.15
  122.7 3.5 %all-to-all-start.2 = ((bf16[8,8,352]{2,1,0:T(8,128)(2,1)}), bf16[8,8,352]{2,1,0:T(8,128)(2,1)S(1)}, u32[]{:S(2)}, u32[]{:S(2)}) async-start(bf16[8,8,352]{2,1,0:T(8,128)(2,1)} %fusion.15), calls=%async_computation.2 | async-start | bytes 98304 | tf_op jit(solution)/shard_map/all_to_all | solution.py:159
  127.2 0.7 pad_maximum_fusion
  127.9 3.8 %reshape.276 = bf16[256,8,2,2]{3,2,1,0:T(2,128)(2,1)S(1)} reshape(bf16[256,32]{1,0:T(8,128)(2,1)} %reduce-scatter.4.cloned.1.call-done) | data formatting | bytes 32768
  131.8 1.9 %copy.54 = bf16[8,2,2,256]{3,2,1,0:T(2,128)(2,1)} copy(bf16[8,2,2,256]{2,1,0,3:T(2,128)(2,1)S(1)} %bitcast.75) | data formatting | bytes 32768
  133.7 5.7 %all-to-all-start.1 = ((bf16[8,2,2,256]{3,2,1,0:T(2,128)(2,1)}), bf16[8,2,2,256]{3,2,1,0:T(2,128)(2,1)S(1)}, u32[]{:S(2)}, u32[]{:S(2)}) async-start(bf16[8,2,2,256]{3,2,1,0:T(2,128)(2,1)} %copy.54), calls=%async_computation.1 | async-start | bytes 32768 | tf_op jit(solution)/shard_map/all_to_all | solution.py:140
  139.6 6.4 %all-to-all-done.1 = bf16[8,2,2,256]{3,2,1,0:T(2,128)(2,1)S(1)} async-done(((bf16[8,2,2,256]{3,2,1,0:T(2,128)(2,1)}), bf16[8,2,2,256]{3,2,1,0:T(2,128)(2,1)S(1)}, u32[]{:S(2)}, u32[]{:S(2)}) %all-to-all-start.1) | async-done | bytes 16416 | tf_op jit(solution)/shard_map/all_to_all | solution.py:140
  146.3 1.8 %fusion.47 = (f32[8]{0:T(128)S(1)}, f32[8]{0:T(128)S(1)}, f32[8,256]{1,0:T(8,128)S(1)}) fusion(f32[8,256]{1,0:T(8,128)S(1)} %convolution_add_fusion, bf16[8,2816]{1,0:T(8,128)(2,1)S(1)} %all_to_all.25, bf16[2816,256]{1,0:T(8,128)(2,1)} %all-gather.2.cloned.1.call-done, f32[8]{0:T(128)S(1)} %fusion.22), kind=kOutput, calls=%fused_computation.92 | convolution fusion | flops 11544560 | bytes 1503328 | tf_op jit(solution)/shard_map/dot_general | solution.py:160
  148.2 5.8 %all-reduce = (f32[8]{0:T(128)S(1)}, f32[8]{0:T(128)S(1)}) all-reduce(f32[8]{0:T(128)S(1)} %get-tuple-element.3, f32[8]{0:T(128)S(1)} %get-tuple-element.2), channel_id=1, replica_groups=mesh['ep'=8,'tp'=4] {'tp'}, use_global_device_ids=true, to_apply=%region_15.16 | all-reduce | flops 16 | bytes 128 | tf_op jit(solution)/shard_map/psum | solution.py:169
  153.9 0.7 multiply_convert_fusion.2
  (77 shorter events, 3.1 us)
Async XLA Ops:
  8.0 113.4 %copy-start = (bf16[1024,352]{0,1:T(8,128)(2,1)S(1)}, bf16[1024,352]{0,1:T(8,128)(2,1)}, u32[]{:S(2)}) copy-start(bf16[1024,352]{0,1:T(8,128)(2,1)} %param.35) | copy-start | bytes 2162692
  8.0 26.5 %copy-start.11 = (bf16[8,1,1024,128]{3,2,1,0:T(8,128)(2,1)S(1)}, bf16[8,1,1024,128]{3,2,1,0:T(8,128)(2,1)}, u32[]{:S(2)}) copy-start(bf16[8,1,1024,128]{3,2,1,0:T(8,128)(2,1)} %param.21) | copy-start | bytes 6291460
  11.5 24.3 %copy-start.2 = (bf16[128,1024]{1,0:T(8,128)(2,1)S(1)}, bf16[128,1024]{1,0:T(8,128)(2,1)}, u32[]{:S(2)}) copy-start(bf16[128,1024]{1,0:T(8,128)(2,1)} %param.28) | copy-start | bytes 786436
  11.5 24.3 %copy-start.10 = (f32[128]{0:T(128)S(1)}, f32[128]{0:T(128)}, u32[]{:S(2)}) copy-start(f32[128]{0:T(128)} %param.27) | copy-start | bytes 1540
  11.5 37.2 %copy-start.1 = (bf16[8,1024]{1,0:T(8,128)(2,1)S(1)}, bf16[8,1024]{1,0:T(8,128)(2,1)}, u32[]{:S(2)}) copy-start(bf16[8,1024]{1,0:T(8,128)(2,1)} %param.20) | copy-start | bytes 49156
  11.5 37.5 %copy-start.7 = (f32[1024]{0:T(1024)S(1)}, f32[1024]{0:T(1024)}, u32[]{:S(2)}) copy-start(f32[1024]{0:T(1024)} %param.29) | copy-start | bytes 12292
  50.0 12.7 %all-to-all-start = ((bf16[8,2,2,1024]{3,2,1,0:T(2,128)(2,1)}), bf16[8,2,2,1024]{3,2,1,0:T(2,128)(2,1)S(1)}, u32[]{:S(2)}, u32[]{:S(2)}) async-start(bf16[8,2,2,1024]{3,2,1,0:T(2,128)(2,1)} %reshape_reshape.3), calls=%async_computation | async-start | bytes 131072 | tf_op jit(solution)/shard_map/all_to_all | solution.py:125
  55.8 72.1 %reduce-scatter.4.cloned.1.call-start = ((), (), s32[]{:S(2)}) async-start(), calls=%async_computation.5 | async-start | bytes 327680
  77.5 44.2 %copy-start.12 = (bf16[1024,352]{0,1:T(8,128)(2,1)S(1)}, bf16[1024,352]{0,1:T(8,128)(2,1)}, u32[]{:S(2)}) copy-start(bf16[1024,352]{0,1:T(8,128)(2,1)} %param.36) | copy-start | bytes 2162692
  77.5 48.7 %copy-start.5 = (bf16[1024,16]{0,1:T(8,128)(2,1)S(1)}, bf16[1024,16]{0,1:T(8,128)(2,1)}, u32[]{:S(2)}) copy-start(bf16[1024,16]{0,1:T(8,128)(2,1)} %param.30) | copy-start | bytes 98308
  77.5 48.9 %copy-start.6 = (s32[8,2]{0,1:T(2,128)S(1)}, s32[8,2]{0,1:T(2,128)}, u32[]{:S(2)}) copy-start(s32[8,2]{0,1:T(2,128)} %param.31) | copy-start | bytes 196
  77.6 49.1 %copy-start.8 = (bf16[1024]{0:T(1024)(128)(2,1)S(1)}, bf16[1024]{0:T(1024)(128)(2,1)}, u32[]{:S(2)}) copy-start(bf16[1024]{0:T(1024)(128)(2,1)} %param.38) | copy-start | bytes 6148
  77.6 49.3 %copy-start.3 = (bf16[1024,64]{0,1:T(8,128)(2,1)S(1)}, bf16[1024,64]{0,1:T(8,128)(2,1)}, u32[]{:S(2)}) copy-start(bf16[1024,64]{0,1:T(8,128)(2,1)} %param.25) | copy-start | bytes 393220
  77.6 49.4 %copy-start.4 = (bf16[1024,64]{0,1:T(8,128)(2,1)S(1)}, bf16[1024,64]{0,1:T(8,128)(2,1)}, u32[]{:S(2)}) copy-start(bf16[1024,64]{0,1:T(8,128)(2,1)} %param.24) | copy-start | bytes 393220
  89.9 64.1 %copy-start.9 = (f32[256]{0:T(256)S(1)}, f32[256]{0:T(256)}, u32[]{:S(2)}) copy-start(f32[256]{0:T(256)} %param.39) | copy-start | bytes 3076
  89.9 56.4 %all-gather.2.cloned.1.call-start = ((), (), s32[]{:S(2)}) async-start(), calls=%async_computation.4 | async-start | bytes 1622016 | tf_op jit(solution)/shard_map/all_gather | solution.py:162
  122.7 11.0 %all-to-all-start.2 = ((bf16[8,8,352]{2,1,0:T(8,128)(2,1)}), bf16[8,8,352]{2,1,0:T(8,128)(2,1)S(1)}, u32[]{:S(2)}, u32[]{:S(2)}) async-start(bf16[8,8,352]{2,1,0:T(8,128)(2,1)} %fusion.15), calls=%async_computation.2 | async-start | bytes 98304 | tf_op jit(solution)/shard_map/all_to_all | solution.py:159
  133.7 12.3 %all-to-all-start.1 = ((bf16[8,2,2,256]{3,2,1,0:T(2,128)(2,1)}), bf16[8,2,2,256]{3,2,1,0:T(2,128)(2,1)S(1)}, u32[]{:S(2)}, u32[]{:S(2)}) async-start(bf16[8,2,2,256]{3,2,1,0:T(2,128)(2,1)} %copy.54), calls=%async_computation.1 | async-start | bytes 32768 | tf_op jit(solution)/shard_map/all_to_all | solution.py:140
Sparse Core Ops, SparseCore 0:
  90.0 16.6 reduce-scatter.3
Sparse Core Ops, SparseCore 1:
  92.6 39.9 all-gather.1
where the time goes:
time: 163 us; the launch traced here: 162 us
  blocking collectives  49.4 us (30%)
  local copies, waits for them, and re-layouts  28.6 us (18%)
  other arithmetic  23.6 us (14%)
  between operations  15.8 us (10%)
  matrix products  15.7 us (10%)
  starting transfers between devices  15.2 us (9%)
  waiting for transfers between devices  13.8 us (8%)
    all_gather x1, blocking collectives, body(): shard_rows = lax.all_gather(settled, 'ep', axis=0, tiled=True)  30.9 us
    unnamed x33, local copies, waits for them, and re-layouts  26.8 us
    another operation x2, other arithmetic  20.1 us
    psum x1, blocking collectives, body(): lax.psum(partial_out.astype(jnp.bfloat16), 'tp').astype(jnp.float32)  12.7 us
    all_to_all x1, waiting for transfers between devices, body(): lax.all_to_all(outgoing, 'ep', split_axis=0, concat_axis=0, tiled=True)  6.8 us
    all_to_all x1, waiting for transfers between devices, body(): lax.all_to_all(summed.astype(jnp.bfloat16), 'ep', split_axis=0, concat_ax...  6.44 us
    all_to_all x1, starting transfers between devices, body(): lax.all_to_all(outgoing, 'ep', split_axis=0, concat_axis=0, tiled=True)  5.81 us
    psum x1, blocking collectives, body(): lax.psum((jnp.sum(combined, axis=1), jnp.sum(combined * combined, axis=1)...  5.76 us
  transfers between devices with their start and end apart: 5, of which 2 were waited for; matrix products, arithmetic and copies ran while one was open for 6% of the time, Pallas kernels for 0%

commit v1 on v0

--- a/solution.py
+++ b/solution.py
@@ -1,6 +1,10 @@
+import functools
+
 import jax
 import jax.numpy as jnp
 from jax import lax
+from jax.experimental import pallas as pl
+from jax.experimental.pallas import tpu as pltpu
 from jax.sharding import PartitionSpec as P
 
 FE = 3584
@@ -177,6 +181,457 @@
     return (result, new_kv)
 
 
+LANES = 128
+HBM_ARGS = (
+    "tokens",
+    "w_query",
+    "kv_cache",
+    "w_key",
+    "w_value",
+    "head_gain",
+    "w_output",
+    "attn_norm_gain",
+    "w_router",
+    "routes",
+    "mix_gate",
+    "expert_gate",
+    "expert_up",
+    "dense_gate",
+    "dense_up",
+    "dense_down",
+    "expert_down",
+    "ffn_norm_gain",
+)
+
+
+def silu(values):
+    return values / (1.0 + jnp.exp(-values))
+
+
+def layer_kernel(sizes, *refs):
+    ep, tp = sizes
+    count = len(HBM_ARGS)
+    lengths_ref, bias_ref = refs[:2]
+    hbm = dict(zip(HBM_ARGS, refs[2 : 2 + count]))
+    out_ref, new_kv_ref = refs[2 + count : 4 + count]
+    vmem = dict(zip(HBM_ARGS, refs[4 + count : 4 + 2 * count]))
+    (
+        parts,
+        rows,
+        mixes,
+        stacked,
+        hidden,
+        outgoing,
+        incoming,
+        stats,
+        load_sem,
+        kv_sem,
+        part_send,
+        part_recv,
+        row_send,
+        row_recv,
+        mix_send,
+        mix_recv,
+        block_send,
+        block_recv,
+        stat_send,
+        stat_recv,
+    ) = refs[4 + 2 * count :]
+    e = lax.axis_index("ep")
+    t = lax.axis_index("tp")
+    seqs, width = vmem["tokens"].shape
+    positions, kv_width = vmem["kv_cache"].shape[1:]
+    head_dim = kv_width // 2
+    experts = vmem["w_router"].shape[1]
+    columns = vmem["expert_gate"].shape[1]
+    slice_width = width // tp
+    devices = ep * tp
+    me = e * tp + t
+
+    barrier = pltpu.get_barrier_semaphore()
+
+    def greet(k, carry):
+        peer = lax.rem(me + k, devices)
+        pl.semaphore_signal(
+            barrier,
+            inc=1,
+            device_id=(peer // tp, lax.rem(peer, tp)),
+            device_id_type=pl.DeviceIdType.MESH,
+        )
+        return carry
+
+    def load(name):
+        return pltpu.make_async_copy(hbm[name], vmem[name], load_sem.at[HBM_ARGS.index(name)])
+
+    def load_kv(b):
+        return pltpu.make_async_copy(
+            hbm["kv_cache"].at[b, 0], vmem["kv_cache"].at[b], kv_sem.at[b]
+        )
+
+    for name in HBM_ARGS:
+        if name == "kv_cache":
+            for b in range(seqs):
+                load_kv(b).start()
+        else:
+            load(name).start()
+    lax.fori_loop(1, devices, greet, 0)
+
+    load("tokens").wait()
+    load("w_query").wait()
+    tokens = vmem["tokens"][...]
+    queries = jnp.dot(tokens, vmem["w_query"][...], preferred_element_type=jnp.float32)
+    queries = queries.astype(jnp.bfloat16).astype(jnp.float32)
+    lane = lax.broadcasted_iota(jnp.int32, (1, kv_width), 1)
+    stack = jnp.concatenate([queries, pltpu.roll(queries, head_dim, 1)], axis=0)
+    stack = jnp.where(lane < head_dim, stack, 0.0)
+    pairs = stack.shape[0]
+    row = lax.broadcasted_iota(jnp.int32, (pairs, 1), 0)
+    owner = lax.rem(row, seqs)
+    scores = jnp.zeros((pairs, positions), jnp.float32)
+    for b in range(seqs):
+        load_kv(b).wait()
+        own = jnp.where(owner == b, stack, 0.0).astype(jnp.bfloat16)
+        scores += lax.dot_general(
+            own,
+            vmem["kv_cache"][b],
+            (((1,), (1,)), ((), ())),
+            preferred_element_type=jnp.float32,
+        )
+    limit = jnp.zeros((pairs, 1), jnp.int32)
+    for b in range(seqs):
+        limit = jnp.where(owner == b, lengths_ref[b], limit)
+    bias = jnp.where(row < seqs, bias_ref[0], bias_ref[1])
+    z = scores * head_dim ** (-0.5) + bias
+    visible = lax.broadcasted_iota(jnp.int32, (pairs, positions), 1) < limit
+    tail = jnp.log1p(jnp.exp(-jnp.abs(z)))
+    survive = jnp.where(visible, -(jnp.maximum(z, 0.0) + tail), 0.0)
+    blocks = positions // LANES
+    tall = jnp.concatenate(
+        [survive[:, j * LANES : (j + 1) * LANES] for j in range(blocks)], axis=0
+    )
+    high = tall.astype(jnp.bfloat16)
+    rest = tall - high.astype(jnp.float32)
+    middle = rest.astype(jnp.bfloat16)
+    low = (rest - middle.astype(jnp.float32)).astype(jnp.bfloat16)
+    later = (
+        lax.broadcasted_iota(jnp.int32, (LANES, LANES), 0)
+        > lax.broadcasted_iota(jnp.int32, (LANES, LANES), 1)
+    ).astype(jnp.float32).astype(jnp.bfloat16)
+    sums = jnp.dot(
+        jnp.concatenate([high, middle, low], axis=0), later, preferred_element_type=jnp.float32
+    )
+    height = blocks * pairs
+    sums = sums[:height] + sums[height : 2 * height] + sums[2 * height :]
+    totals = jnp.sum(tall, axis=1, keepdims=True)
+    running = jnp.zeros((pairs, 1), jnp.float32)
+    pieces = [None] * blocks
+    for j in reversed(range(blocks)):
+        pieces[j] = sums[j * pairs : (j + 1) * pairs] + running
+        running = running + totals[j * pairs : (j + 1) * pairs]
+    remaining = jnp.concatenate(pieces, axis=1)
+    weights = jnp.where(visible, jnp.exp(jnp.minimum(z, 0.0) - tail + remaining), 0.0)
+    blended = jnp.zeros((pairs, kv_width), jnp.float32)
+    for b in range(seqs):
+        own = jnp.where(owner == b, weights, 0.0).astype(jnp.bfloat16)
+        blended += jnp.dot(own, vmem["kv_cache"][b], preferred_element_type=jnp.float32)
+    blended = jnp.where(lane >= head_dim, blended, 0.0)
+    spread = jnp.sum(blended * blended, axis=1, keepdims=True) / head_dim
+    blended = blended * lax.rsqrt(spread + 1e-06)
+    load("head_gain").wait()
+    normed = pltpu.roll(blended[:seqs], head_dim, 1) + blended[seqs:]
+    normed = (normed * vmem["head_gain"][...]).astype(jnp.bfloat16)
+    load("w_output").wait()
+    partial = jnp.dot(normed, vmem["w_output"][...], preferred_element_type=jnp.float32)
+    parts[t] = partial.astype(jnp.bfloat16)
+
+    pl.semaphore_wait(barrier, devices - 1)
+
+    def to_tp(buffer, send, recv, peer, slot):
+        return pltpu.make_async_remote_copy(
+            src_ref=buffer.at[slot],
+            dst_ref=buffer.at[slot],
+            send_sem=send.at[peer],
+            recv_sem=recv.at[slot],
+            device_id=(e, peer),
+            device_id_type=pl.DeviceIdType.MESH,
+        )
+
+    def to_ep(buffer, send, recv, peer, slot):
+        return pltpu.make_async_remote_copy(
+            src_ref=buffer.at[slot],
+            dst_ref=buffer.at[slot],
+            send_sem=send.at[peer],
+            recv_sem=recv.at[slot],
+            device_id=(peer, t),
+            device_id_type=pl.DeviceIdType.MESH,
+        )
+
+    def tp_peer(k):
+        return lax.rem(t + k, tp)
+
+    def ep_peer(k):
+        return lax.rem(e + k, ep)
+
+    for k in range(1, tp):
+        to_tp(parts, part_send, part_recv, tp_peer(k), t).start()
+
+    load("w_key").wait()
+    load("w_value").wait()
+    key_new = jnp.dot(tokens, vmem["w_key"][...], preferred_element_type=jnp.float32)
+    value_new = jnp.dot(tokens, vmem["w_value"][...], preferred_element_type=jnp.float32)
+    new_kv_ref[...] = jnp.concatenate([key_new, value_new], axis=1).astype(jnp.bfloat16)
+
+    load("attn_norm_gain").wait()
+    for k in range(1, tp):
+        to_tp(parts, part_send, part_recv, tp_peer(k), tp_peer(k)).wait_recv()
+    attended = jnp.sum(parts[...].astype(jnp.float32), axis=0)
+    settled = layer_norm(
+        RESIDUAL_SCALE * tokens.astype(jnp.float32) + attended, vmem["attn_norm_gain"][...]
+    ).astype(jnp.bfloat16)
+    rows[e] = settled
+    for k in range(1, ep):
+        to_ep(rows, row_send, row_recv, ep_peer(k), e).start()
+
+    load("w_router").wait()
+    load("routes").wait()
+    load("mix_gate").wait()
+    logits = jnp.dot(settled, vmem["w_router"][...], preferred_element_type=jnp.float32)
+    expert_lane = lax.broadcasted_iota(jnp.int32, (seqs, experts), 1)
+    routes = vmem["routes"][...]
+    first, second = routes[:, :1], routes[:, 1:2]
+    first_logit = jnp.sum(jnp.where(expert_lane == first, logits, 0.0), axis=1, keepdims=True)
+    second_logit = jnp.sum(jnp.where(expert_lane == second, logits, 0.0), axis=1, keepdims=True)
+    settled_wide = settled.astype(jnp.float32)
+    mix = jax.nn.sigmoid(
+        jnp.sum(settled_wide * vmem["mix_gate"][...].astype(jnp.float32), axis=1, keepdims=True)
+    )
+    wide_lane = lax.broadcasted_iota(jnp.int32, (seqs, LANES), 1)
+    mixes[e] = (
+        jnp.where(wide_lane == first, jax.nn.sigmoid(first_logit - second_logit), 0.0)
+        + jnp.where(wide_lane == second, jax.nn.sigmoid(second_logit - first_logit), 0.0)
+        + jnp.where(wide_lane == experts, mix, 0.0)
+    )
+    for k in range(1, ep):
+        to_ep(mixes, mix_send, mix_recv, ep_peer(k), e).start()
+
+    for name in ("expert_gate", "expert_up", "dense_gate", "dense_up", "dense_down"):
+        load(name).wait()
+    for k in range(1, ep):
+        to_ep(rows, row_send, row_recv, ep_peer(k), ep_peer(k)).wait_recv()
+    stacked[...] = jnp.concatenate(
+        [rows[i].astype(jnp.float32) for i in range(ep)], axis=0
+    ).astype(jnp.bfloat16)
+
+    tile = 256 if columns % 256 == 0 else LANES
+
+    def up_tile(i, carry):
+        at = pl.ds(pl.multiple_of(i * tile, tile), tile)
+        gate_pre = jnp.dot(
+            stacked[...], vmem["expert_gate"][:, at], preferred_element_type=jnp.float32
+        )
+        up_pre = jnp.dot(
+            stacked[...], vmem["expert_up"][:, at], preferred_element_type=jnp.float32
+        )
+        hidden[:, at] = (silu(gate_pre) * up_pre).astype(jnp.bfloat16)
+        return carry
+
+    lax.fori_loop(0, columns // tile, up_tile, 0)
+    gate_pre = jnp.dot(
+        stacked[...], vmem["dense_gate"][...], preferred_element_type=jnp.float32
+    )
+    up_pre = jnp.dot(stacked[...], vmem["dense_up"][...], preferred_element_type=jnp.float32)
+    dense_hidden = (silu(gate_pre) * up_pre).astype(jnp.bfloat16)
+    dense = jnp.dot(dense_hidden, vmem["dense_down"][...], preferred_element_type=jnp.float32)
+
+    for k in range(1, ep):
+        to_ep(mixes, mix_send, mix_recv, ep_peer(k), ep_peer(k)).wait_recv()
+    table = mixes[...].reshape(ep * seqs, LANES)
+    own_expert = me * experts // devices
+    all_lane = lax.broadcasted_iota(jnp.int32, (ep * seqs, LANES), 1)
+    expert_weight = jnp.sum(jnp.where(all_lane == own_expert, table, 0.0), axis=1, keepdims=True)
+    dense_weight = jnp.sum(jnp.where(all_lane == experts, table, 0.0), axis=1, keepdims=True)
+    dense = dense * dense_weight
+
+    def block_copy(source, target, send_slot, recv_slot, to_e, to_t):
+        return pltpu.make_async_remote_copy(
+            src_ref=outgoing.at[source],
+            dst_ref=incoming.at[target],
+            send_sem=block_send.at[send_slot],
+            recv_sem=block_recv.at[recv_slot],
+            device_id=(to_e, to_t),
+            device_id_type=pl.DeviceIdType.MESH,
+        )
+
+    load("expert_down").wait()
+    for j in range(tp):
+        value = jnp.dot(
+            hidden[...],
+            vmem["expert_down"][:, j * slice_width : (j + 1) * slice_width],
+            preferred_element_type=jnp.float32,
+        )
+        value = value * expert_weight + jnp.where(t == j, dense, 0.0)
+        for i in range(ep):
+            outgoing[i * tp + j] = value[i * seqs : (i + 1) * seqs].astype(jnp.bfloat16)
+
+        def send_block(k, carry, j=j):
+            to_e = ep_peer(k)
+            peer = to_e * tp + j
+
+            @pl.when(peer != me)
+            def _():
+                block_copy(peer, me, peer, me, to_e, j).start()
+
+            return carry
+
+        lax.fori_loop(0, ep, send_block, 0)
+    incoming[me] = outgoing[me]
+    load("ffn_norm_gain").wait()
+
+    def wait_block(k, carry):
+        peer = lax.rem(me + k, devices)
+        block_copy(peer, peer, peer, peer, peer // tp, lax.rem(peer, tp)).wait_recv()
+        return carry
+
+    lax.fori_loop(1, devices, wait_block, 0)
+    combined = jnp.sum(incoming[...].astype(jnp.float32), axis=0)
+    mine = jnp.zeros((seqs, slice_width), jnp.float32)
+    for j in range(tp):
+        mine = jnp.where(t == j, settled_wide[:, j * slice_width : (j + 1) * slice_width], mine)
+    combined = combined + RESIDUAL_SCALE * mine
+    row_sum = jnp.sum(combined, axis=1, keepdims=True)
+    square = jnp.sum(combined * combined, axis=1, keepdims=True)
+    stats[t] = jnp.where(wide_lane == 0, row_sum, jnp.where(wide_lane == 1, square, 0.0))
+    for k in range(1, tp):
+        to_tp(stats, stat_send, stat_recv, tp_peer(k), t).start()
+    for k in range(1, tp):
+        to_tp(stats, stat_send, stat_recv, tp_peer(k), tp_peer(k)).wait_recv()
+    both = jnp.sum(stats[...], axis=0)
+    row_mean = both[:, :1] / width
+    row_var = both[:, 1:2] / width - row_mean * row_mean
+    out_ref[...] = (
+        (combined - row_mean) * lax.rsqrt(row_var + 1e-05) * vmem["ffn_norm_gain"][...]
+    ).astype(jnp.bfloat16)
+
+    for k in range(1, tp):
+        to_tp(parts, part_send, part_recv, tp_peer(k), t).wait_send()
+        to_tp(stats, stat_send, stat_recv, tp_peer(k), t).wait_send()
+    for k in range(1, ep):
+        to_ep(rows, row_send, row_recv, ep_peer(k), e).wait_send()
+        to_ep(mixes, mix_send, mix_recv, ep_peer(k), e).wait_send()
+
+    def drain(k, carry):
+        peer = lax.rem(me + k, devices)
+        block_copy(peer, me, peer, me, peer // tp, lax.rem(peer, tp)).wait_send()
+        return carry
+
+    lax.fori_loop(1, devices, drain, 0)
+
+
+NAMES = (
+    "tokens",
+    "kv_cache",
+    "lengths",
+    "w_query",
+    "w_key",
+    "w_value",
+    "break_bias",
+    "head_gain",
+    "w_output",
+    "attn_norm_gain",
+    "w_router",
+    "routes",
+    "expert_gate",
+    "expert_up",
+    "expert_down",
+    "dense_gate",
+    "dense_up",
+    "dense_down",
+    "mix_gate",
+    "ffn_norm_gain",
+)
+
+
+def fused_fits(args, ep, tp):
+    seqs, width = args["tokens"].shape
+    _, key_heads, positions, kv_width = args["kv_cache"].shape
+    experts = args["w_router"].shape[1]
+    return (
+        seqs == 8
+        and key_heads == 1
+        and kv_width == LANES
+        and args["w_query"].shape[1] == LANES
+        and positions % LANES == 0
+        and experts < LANES
+        and args["routes"].shape[1] == 2
+        and (ep * tp) % experts == 0
+        and args["expert_gate"].shape[1] % LANES == 0
+        and (width // tp) % LANES == 0
+    )
+
+
+def fused(args, ep, tp):
+    for name in ("head_gain", "attn_norm_gain", "mix_gate", "ffn_norm_gain"):
+        args[name] = args[name].reshape(1, -1)
+    operands = [args[name] for name in HBM_ARGS]
+    seqs, width = args["tokens"].shape
+    slice_width = width // tp
+    devices = ep * tp
+    scratch = []
+    for name, operand in zip(HBM_ARGS, operands):
+        shape = operand.shape
+        if name == "kv_cache":
+            shape = (shape[0],) + shape[2:]
+        scratch.append(pltpu.VMEM(shape, operand.dtype))
+    dma = pltpu.SemaphoreType.DMA
+    scratch += [
+        pltpu.VMEM((tp, seqs, width), jnp.bfloat16),
+        pltpu.VMEM((ep, seqs, width), jnp.bfloat16),
+        pltpu.VMEM((ep, seqs, LANES), jnp.float32),
+        pltpu.VMEM((ep * seqs, width), jnp.bfloat16),
+        pltpu.VMEM((ep * seqs, args["expert_gate"].shape[1]), jnp.bfloat16),
+        pltpu.VMEM((devices, seqs, slice_width), jnp.bfloat16),
+        pltpu.VMEM((devices, seqs, slice_width), jnp.bfloat16),
+        pltpu.VMEM((tp, seqs, LANES), jnp.float32),
+        dma((len(HBM_ARGS),)),
+        dma((seqs,)),
+        dma((tp,)),
+        dma((tp,)),
+        dma((ep,)),
+        dma((ep,)),
+        dma((ep,)),
+        dma((ep,)),
+        dma((devices,)),
+        dma((devices,)),
+        dma((tp,)),
+        dma((tp,)),
+    ]
+    smem = pl.BlockSpec(memory_space=pltpu.SMEM)
+    result, new_kv = pl.pallas_call(
+        functools.partial(layer_kernel, (ep, tp)),
+        out_shape=(
+            jax.ShapeDtypeStruct((seqs, slice_width), jnp.bfloat16),
+            jax.ShapeDtypeStruct((seqs, LANES), jnp.bfloat16),
+        ),
+        in_specs=[smem, smem] + [pl.BlockSpec(memory_space=pl.ANY)] * len(HBM_ARGS),
+        out_specs=(
+            pl.BlockSpec(memory_space=pltpu.VMEM),
+            pl.BlockSpec(memory_space=pltpu.VMEM),
+        ),
+        scratch_shapes=scratch,
+        compiler_params=pltpu.CompilerParams(
+            collective_id=0, has_side_effects=True, vmem_limit_bytes=60 * 1024 * 1024
+        ),
+    )(args["lengths"], args["break_bias"], *operands)
+    return result, new_kv.reshape(seqs, 1, LANES)
+
+
+def layer(ep, tp, *arrays):
+    args = dict(zip(NAMES, arrays))
+    if fused_fits(args, ep, tp):
+        return fused(args, ep, tp)
+    return body(*arrays)
+
+
 def solution(mesh):
     in_specs = (
         P("ep", None),
@@ -201,4 +656,5 @@
         P("tp"),
     )
     out_specs = (P("ep", "tp"), P("ep", "tp", None))
-    return jax.shard_map(body, mesh=mesh, in_specs=in_specs, out_specs=out_specs, check_vma=False)
+    step = functools.partial(layer, mesh.shape["ep"], mesh.shape["tp"])
+    return jax.shard_map(step, mesh=mesh, in_specs=in_specs, out_specs=out_specs, check_vma=False)

time: 163 us -> 47.8 us (0.29)
  blocking collectives: 49.4 us -> 0 us
  Pallas kernels: 0 us -> 31.9 us
  other arithmetic: 23.6 us -> 0 us
  matrix products: 15.7 us -> 0 us
  starting transfers between devices: 15.2 us -> 0 us
  between operations: 15.8 us -> 0.64 us
  local copies, waits for them, and re-layouts: 28.6 us -> 14.8 us
  waiting for transfers between devices: 13.8 us -> 0 us
    pallas_call x0 -> x1, Pallas kernels: none -> 31.9 us  [fused(): pl.pallas_call(functools.partial(layer_kernel, (ep, tp)), out_shape=(jax....]
    all_gather x1 -> x0, blocking collectives: 30.9 us -> none  [body(): shard_rows = lax.all_gather(settled, 'ep', axis=0, tiled=True)]
    another operation x3 -> x0, other arithmetic: 20.2 us -> none
    psum x2 -> x0, blocking collectives: 18.5 us -> none  [the longest x1 12.7 us: body(): lax.psum(partial_out.astype(jnp.bfloat16), 'tp').astype(jnp.float32)]
    dot_general x16 -> x0, matrix products: 15.7 us -> none  [the longest x1 4.22 us: body(): jnp.dot(hidden, expert_down, preferred_element_type=jnp.float32)]
    all_to_all x3 -> x0, starting transfers between devices: 15.1 us -> none  [the longest x1 5.81 us: body(): lax.all_to_all(outgoing, 'ep', split_axis=0, concat_axis=0, tiled=True)]
    unnamed x33 -> x8, local copies, waits for them, and re-layouts: 26.8 us -> 13.5 us
    all_to_all x3 -> x0, waiting for transfers between devices: 13.2 us -> none  [the longest x1 6.8 us: body(): lax.all_to_all(outgoing, 'ep', split_axis=0, concat_axis=0, tiled=True)]
  transfers between devices with their start and end apart: 5 -> 0, of which waited for: 2 -> 0; matrix products, arithmetic and copies ran while one was open for 6% -> 0% of each run, Pallas kernels for 0% -> 0%
where the time goes in v1:
time: 47.8 us; the launch traced here: 47.4 us
  Pallas kernels  31.9 us (67%)
  local copies, waits for them, and re-layouts  14.8 us (31%)
  between operations  0.64 us (1%)
    pallas_call x1, Pallas kernels, fused(): pl.pallas_call(functools.partial(layer_kernel, (ep, tp)), out_shape=(jax....  31.9 us
    unnamed x8, local copies, waits for them, and re-layouts  13.5 us
    reshape x1, local copies, waits for them, and re-layouts, fused(): args[name] = args[name].reshape(1, -1)  1.27 us

profile of v1, /device:TPU:0, one launch (start us, length us, event | category | flops | bytes accessed | tf_op | source)
XLA Modules:
  0.0 47.4 jit_solution(3222723755214939178)
XLA Ops:
  0.6 1.3 %copy.25.refs_11_ = s32[8,2]{1,0:T(8,128)} copy(s32[8,2]{0,1:T(2,128)} %param.31) | data formatting | bytes 128 | tf_op args[11]
  2.0 1.3 %reshape.21.refs_12_ = bf16[1,1024]{1,0:T(2,128)(2,1)} reshape(bf16[1024]{0:T(1024)(128)(2,1)} %param.38) | data formatting | bytes 4096 | tf_op jit(solution)/shard_map/reshape | solution.py:574
  3.2 1.7 %copy.22.refs_5_ = bf16[1024,64]{1,0:T(8,128)(2,1)} copy(bf16[1024,64]{0,1:T(8,128)(2,1)} %param.24) | data formatting | bytes 262144 | tf_op args[4]
  5.0 1.7 %copy.23.refs_6_ = bf16[1024,64]{1,0:T(8,128)(2,1)} copy(bf16[1024,64]{0,1:T(8,128)(2,1)} %param.25) | data formatting | bytes 262144 | tf_op args[5]
  6.7 1.6 %copy.24.refs_10_ = bf16[1024,16]{1,0:T(8,128)(2,1)} copy(bf16[1024,16]{0,1:T(8,128)(2,1)} %param.30) | data formatting | bytes 65536 | tf_op args[10]
  8.4 2.3 %copy.26.refs_15_ = bf16[1024,352]{1,0:T(8,128)(2,1)} copy(bf16[1024,352]{0,1:T(8,128)(2,1)} %param.35) | data formatting | bytes 1441792 | tf_op args[15]
  10.6 2.3 %copy.27.refs_16_ = bf16[1024,352]{1,0:T(8,128)(2,1)} copy(bf16[1024,352]{0,1:T(8,128)(2,1)} %param.36) | data formatting | bytes 1441792 | tf_op args[16]
  12.9 31.9 %shard_map.203 = (bf16[8,256]{1,0:T(8,128)(2,1)}, bf16[8,128]{1,0:T(8,128)(2,1)}) custom-call(s32[8]{0:T(128)} %refs_0_.1, f32[2]{0:T(128)} %refs_1_.1, bf16[8,1024]{1,0:T(8,128)(2,1)} %refs_2_.1, bf16[1024,128]{1,0:T(8,128)(2,1)} %refs_3_.1, bf16[8,1,1024,128]{3,2,1,0:T(8,128)(2,1)} %refs_4_.1, bf16[1024,64]{1,0:T(8,128)(2,1)} %copy.22.refs_5_, ...), custom_call_target="tpu_custom_call" | custom-call | tf_op jit(solution)/shard_map/pallas_call | solution.py:609
  44.8 1.3 %copy.30 = bf16[8,256]{1,0:T(8,128)(2,1)} copy(bf16[8,256]{1,0:T(8,128)(2,1)} %get-tuple-element.8) | data formatting | bytes 8192
  46.1 1.2 %copy.31 = bf16[8,1,128]{2,0,1:T(8,128)(2,1)} copy(bf16[8,1,128]{2,0,1:T(8,128)(2,1)} %bitcast.5) | data formatting | bytes 4096

commit v2 on v1

--- a/solution.py
+++ b/solution.py
@@ -192,7 +192,6 @@
     "w_output",
     "attn_norm_gain",
     "w_router",
-    "routes",
     "mix_gate",
     "expert_gate",
     "expert_up",
@@ -208,13 +207,19 @@
     return values / (1.0 + jnp.exp(-values))
 
 
+def dot_rows(left, right):
+    return lax.dot_general(
+        left, right, (((1,), (1,)), ((), ())), preferred_element_type=jnp.float32
+    )
+
+
 def layer_kernel(sizes, *refs):
     ep, tp = sizes
     count = len(HBM_ARGS)
-    lengths_ref, bias_ref = refs[:2]
-    hbm = dict(zip(HBM_ARGS, refs[2 : 2 + count]))
-    out_ref, new_kv_ref = refs[2 + count : 4 + count]
-    vmem = dict(zip(HBM_ARGS, refs[4 + count : 4 + 2 * count]))
+    lengths_ref, bias_ref, routes_ref = refs[:3]
+    hbm = dict(zip(HBM_ARGS, refs[3 : 3 + count]))
+    out_ref, new_kv_ref = refs[3 + count : 5 + count]
+    vmem = dict(zip(HBM_ARGS, refs[5 + count : 5 + 2 * count]))
     (
         parts,
         rows,
@@ -236,13 +241,13 @@
         block_recv,
         stat_send,
         stat_recv,
-    ) = refs[4 + 2 * count :]
+    ) = refs[5 + 2 * count :]
     e = lax.axis_index("ep")
     t = lax.axis_index("tp")
     seqs, width = vmem["tokens"].shape
     positions, kv_width = vmem["kv_cache"].shape[1:]
     head_dim = kv_width // 2
-    experts = vmem["w_router"].shape[1]
+    experts = vmem["w_router"].shape[0]
     columns = vmem["expert_gate"].shape[1]
     slice_width = width // tp
     devices = ep * tp
@@ -291,12 +296,7 @@
     for b in range(seqs):
         load_kv(b).wait()
         own = jnp.where(owner == b, stack, 0.0).astype(jnp.bfloat16)
-        scores += lax.dot_general(
-            own,
-            vmem["kv_cache"][b],
-            (((1,), (1,)), ((), ())),
-            preferred_element_type=jnp.float32,
-        )
+        scores += dot_rows(own, vmem["kv_cache"][b])
     limit = jnp.zeros((pairs, 1), jnp.int32)
     for b in range(seqs):
         limit = jnp.where(owner == b, lengths_ref[b], limit)
@@ -377,8 +377,8 @@
 
     load("w_key").wait()
     load("w_value").wait()
-    key_new = jnp.dot(tokens, vmem["w_key"][...], preferred_element_type=jnp.float32)
-    value_new = jnp.dot(tokens, vmem["w_value"][...], preferred_element_type=jnp.float32)
+    key_new = dot_rows(tokens, vmem["w_key"][...])
+    value_new = dot_rows(tokens, vmem["w_value"][...])
     new_kv_ref[...] = jnp.concatenate([key_new, value_new], axis=1).astype(jnp.bfloat16)
 
     load("attn_norm_gain").wait()
@@ -393,18 +393,23 @@
         to_ep(rows, row_send, row_recv, ep_peer(k), e).start()
 
     load("w_router").wait()
-    load("routes").wait()
     load("mix_gate").wait()
-    logits = jnp.dot(settled, vmem["w_router"][...], preferred_element_type=jnp.float32)
+    logits = dot_rows(settled, vmem["w_router"][...])
     expert_lane = lax.broadcasted_iota(jnp.int32, (seqs, experts), 1)
-    routes = vmem["routes"][...]
-    first, second = routes[:, :1], routes[:, 1:2]
+    seq_row = lax.broadcasted_iota(jnp.int32, (seqs, 1), 0)
+    first = jnp.zeros((seqs, 1), jnp.int32)
+    second = jnp.zeros((seqs, 1), jnp.int32)
+    for b in range(seqs):
+        first = jnp.where(seq_row == b, routes_ref[0, b], first)
+        second = jnp.where(seq_row == b, routes_ref[1, b], second)
     first_logit = jnp.sum(jnp.where(expert_lane == first, logits, 0.0), axis=1, keepdims=True)
     second_logit = jnp.sum(jnp.where(expert_lane == second, logits, 0.0), axis=1, keepdims=True)
     settled_wide = settled.astype(jnp.float32)
-    mix = jax.nn.sigmoid(
-        jnp.sum(settled_wide * vmem["mix_gate"][...].astype(jnp.float32), axis=1, keepdims=True)
-    )
+    mix_gate = vmem["mix_gate"][...].astype(jnp.float32)
+    products = jnp.zeros((seqs, LANES), jnp.float32)
+    for j in range(width // LANES):
+        products += settled_wide[:, j * LANES : (j + 1) * LANES] * mix_gate[j : j + 1]
+    mix = jax.nn.sigmoid(jnp.sum(products, axis=1, keepdims=True))
     wide_lane = lax.broadcasted_iota(jnp.int32, (seqs, LANES), 1)
     mixes[e] = (
         jnp.where(wide_lane == first, jax.nn.sigmoid(first_logit - second_logit), 0.0)
@@ -436,10 +441,8 @@
         return carry
 
     lax.fori_loop(0, columns // tile, up_tile, 0)
-    gate_pre = jnp.dot(
-        stacked[...], vmem["dense_gate"][...], preferred_element_type=jnp.float32
-    )
-    up_pre = jnp.dot(stacked[...], vmem["dense_up"][...], preferred_element_type=jnp.float32)
+    gate_pre = dot_rows(stacked[...], vmem["dense_gate"][...])
+    up_pre = dot_rows(stacked[...], vmem["dense_up"][...])
     dense_hidden = (silu(gate_pre) * up_pre).astype(jnp.bfloat16)
     dense = jnp.dot(dense_hidden, vmem["dense_down"][...], preferred_element_type=jnp.float32)
 
@@ -525,6 +528,11 @@
         return carry
 
     lax.fori_loop(1, devices, drain, 0)
+
+
+def finish_kernel(result_ref, new_kv_ref, result_out, new_kv_out):
+    result_out[...] = result_ref[...]
+    new_kv_out[...] = new_kv_ref[...]
 
 
 NAMES = (
@@ -570,8 +578,11 @@
 
 
 def fused(args, ep, tp):
-    for name in ("head_gain", "attn_norm_gain", "mix_gate", "ffn_norm_gain"):
+    for name in ("head_gain", "attn_norm_gain", "ffn_norm_gain"):
         args[name] = args[name].reshape(1, -1)
+    args["mix_gate"] = args["mix_gate"].reshape(-1, LANES)
+    for name in ("w_key", "w_value", "w_router", "routes", "dense_gate", "dense_up"):
+        args[name] = args[name].T
     operands = [args[name] for name in HBM_ARGS]
     seqs, width = args["tokens"].shape
     slice_width = width // tp
@@ -612,7 +623,7 @@
             jax.ShapeDtypeStruct((seqs, slice_width), jnp.bfloat16),
             jax.ShapeDtypeStruct((seqs, LANES), jnp.bfloat16),
         ),
-        in_specs=[smem, smem] + [pl.BlockSpec(memory_space=pl.ANY)] * len(HBM_ARGS),
+        in_specs=[smem, smem, smem] + [pl.BlockSpec(memory_space=pl.ANY)] * len(HBM_ARGS),
         out_specs=(
             pl.BlockSpec(memory_space=pltpu.VMEM),
             pl.BlockSpec(memory_space=pltpu.VMEM),
@@ -621,7 +632,14 @@
         compiler_params=pltpu.CompilerParams(
             collective_id=0, has_side_effects=True, vmem_limit_bytes=60 * 1024 * 1024
         ),
-    )(args["lengths"], args["break_bias"], *operands)
+    )(args["lengths"], args["break_bias"], args["routes"], *operands)
+    result, new_kv = pl.pallas_call(
+        finish_kernel,
+        out_shape=(
+            jax.ShapeDtypeStruct(result.shape, result.dtype),
+            jax.ShapeDtypeStruct(new_kv.shape, new_kv.dtype),
+        ),
+    )(result, new_kv)
     return result, new_kv.reshape(seqs, 1, LANES)
 
 

time: 47.8 us -> 34.1 us (0.71)
  local copies, waits for them, and re-layouts: 14.8 us -> 0 us
  Pallas kernels: 31.9 us -> 33.2 us
    unnamed x8 -> x0, local copies, waits for them, and re-layouts: 13.5 us -> none
    reshape x1 -> x0, local copies, waits for them, and re-layouts: 1.27 us -> none  [fused(): args[name] = args[name].reshape(1, -1)]
    pallas_call x0 -> x1, Pallas kernels: none -> 1.27 us  [fused(): pl.pallas_call(finish_kernel, out_shape=(jax.ShapeDtypeStruct(result.shap...]
where the time goes in v2:
time: 34.1 us; the launch traced here: 33.8 us
  Pallas kernels  33.2 us (97%)
  between operations  0.65 us (2%)
    pallas_call x1, Pallas kernels, fused(): pl.pallas_call(functools.partial(layer_kernel, (ep, tp)), out_shape=(jax....  31.9 us
    pallas_call x1, Pallas kernels, fused(): pl.pallas_call(finish_kernel, out_shape=(jax.ShapeDtypeStruct(result.shap...  1.27 us

profile of v2, /device:TPU:0, one launch (start us, length us, event | category | flops | bytes accessed | tf_op | source)
XLA Modules:
  0.0 33.8 jit_solution(10767380878122930543)
XLA Ops:
  0.6 31.9 %shard_map.203 = (bf16[8,256]{1,0:T(8,128)(2,1)}, bf16[8,128]{1,0:T(8,128)(2,1)}) custom-call(s32[8]{0:T(128)} %refs_0_.1, f32[2]{0:T(128)} %refs_1_.1, s32[2,8]{1,0:T(2,128)} %bitcast.18, bf16[8,1024]{1,0:T(8,128)(2,1)} %refs_3_.1, bf16[1024,128]{1,0:T(8,128)(2,1)} %refs_4_.1, bf16[8,1,1024,128]{3,2,1,0:T(8,128)(2,1)} %refs_5_.1, ...), custom_call_target="tpu_custom_call" | custom-call | tf_op jit(solution)/shard_map/pallas_call | solution.py:620
  32.5 1.3 %shard_map.204 = (bf16[8,256]{1,0:T(8,128)(2,1)}, bf16[8,128]{1,0:T(8,128)(2,1)}) custom-call(bf16[8,256]{1,0:T(8,128)(2,1)} %get-tuple-element.6.result_ref, bf16[8,128]{1,0:T(8,128)(2,1)} %get-tuple-element.7.new_kv_ref), custom_call_target="tpu_custom_call" | custom-call | tf_op jit(solution)/shard_map/pallas_call | solution.py:636

commit v3 on v2

--- a/solution.py
+++ b/solution.py
@@ -203,6 +203,10 @@
 )
 
 
+EARLY_ARGS = ("tokens", "w_query")
+LATE_ARGS = tuple(name for name in HBM_ARGS if name not in EARLY_ARGS + ("kv_cache",))
+
+
 def silu(values):
     return values / (1.0 + jnp.exp(-values))
 
@@ -216,7 +220,7 @@
 def layer_kernel(sizes, *refs):
     ep, tp = sizes
     count = len(HBM_ARGS)
-    lengths_ref, bias_ref, routes_ref = refs[:3]
+    scalars_hbm = refs[:3]
     hbm = dict(zip(HBM_ARGS, refs[3 : 3 + count]))
     out_ref, new_kv_ref = refs[3 + count : 5 + count]
     vmem = dict(zip(HBM_ARGS, refs[5 + count : 5 + 2 * count]))
@@ -229,6 +233,10 @@
         outgoing,
         incoming,
         stats,
+        lengths_ref,
+        bias_ref,
+        routes_ref,
+        scalar_sem,
         load_sem,
         kv_sem,
         part_send,
@@ -273,12 +281,18 @@
             hbm["kv_cache"].at[b, 0], vmem["kv_cache"].at[b], kv_sem.at[b]
         )
 
-    for name in HBM_ARGS:
-        if name == "kv_cache":
-            for b in range(seqs):
-                load_kv(b).start()
-        else:
-            load(name).start()
+    scalar_loads = [
+        pltpu.make_async_copy(source, target, scalar_sem.at[i])
+        for i, (source, target) in enumerate(
+            zip(scalars_hbm, (lengths_ref, bias_ref, routes_ref))
+        )
+    ]
+    for name in EARLY_ARGS:
+        load(name).start()
+    for b in range(seqs):
+        load_kv(b).start()
+    for copy in scalar_loads:
+        copy.start()
     lax.fori_loop(1, devices, greet, 0)
 
     load("tokens").wait()
@@ -297,6 +311,10 @@
         load_kv(b).wait()
         own = jnp.where(owner == b, stack, 0.0).astype(jnp.bfloat16)
         scores += dot_rows(own, vmem["kv_cache"][b])
+    for name in LATE_ARGS:
+        load(name).start()
+    for copy in scalar_loads:
+        copy.wait()
     limit = jnp.zeros((pairs, 1), jnp.int32)
     for b in range(seqs):
         limit = jnp.where(owner == b, lengths_ref[b], limit)
@@ -603,6 +621,10 @@
         pltpu.VMEM((devices, seqs, slice_width), jnp.bfloat16),
         pltpu.VMEM((devices, seqs, slice_width), jnp.bfloat16),
         pltpu.VMEM((tp, seqs, LANES), jnp.float32),
+        pltpu.SMEM(args["lengths"].shape, jnp.int32),
+        pltpu.SMEM(args["break_bias"].shape, jnp.float32),
+        pltpu.SMEM(args["routes"].shape, jnp.int32),
+        dma((3,)),
         dma((len(HBM_ARGS),)),
         dma((seqs,)),
         dma((tp,)),
@@ -616,14 +638,13 @@
         dma((tp,)),
         dma((tp,)),
     ]
-    smem = pl.BlockSpec(memory_space=pltpu.SMEM)
     result, new_kv = pl.pallas_call(
         functools.partial(layer_kernel, (ep, tp)),
         out_shape=(
             jax.ShapeDtypeStruct((seqs, slice_width), jnp.bfloat16),
             jax.ShapeDtypeStruct((seqs, LANES), jnp.bfloat16),
         ),
-        in_specs=[smem, smem, smem] + [pl.BlockSpec(memory_space=pl.ANY)] * len(HBM_ARGS),
+        in_specs=[pl.BlockSpec(memory_space=pl.ANY)] * (3 + len(HBM_ARGS)),
         out_specs=(
             pl.BlockSpec(memory_space=pltpu.VMEM),
             pl.BlockSpec(memory_space=pltpu.VMEM),

time: 34.1 us -> 31.5 us (0.924)
  Pallas kernels: 33.2 us -> 30.7 us
    pallas_call x1, Pallas kernels: 31.9 us -> 29.4 us  [fused(): pl.pallas_call(functools.partial(layer_kernel, (ep, tp)), out_shape=(jax....]
where the time goes in v3:
time: 31.5 us; the launch traced here: 31.3 us
  Pallas kernels  30.7 us (97%)
  between operations  0.65 us (2%)
    pallas_call x1, Pallas kernels, fused(): pl.pallas_call(functools.partial(layer_kernel, (ep, tp)), out_shape=(jax....  29.4 us
    pallas_call x1, Pallas kernels, fused(): pl.pallas_call(finish_kernel, out_shape=(jax.ShapeDtypeStruct(result.shap...  1.27 us

profile of v3, /device:TPU:0, one launch (start us, length us, event | category | flops | bytes accessed | tf_op | source)
XLA Modules:
  0.0 31.3 jit_solution(12970708560567543055)
XLA Ops:
  0.6 29.4 %shard_map.203 = (bf16[8,256]{1,0:T(8,128)(2,1)}, bf16[8,128]{1,0:T(8,128)(2,1)}) custom-call(s32[8]{0:T(128)} %refs_0_.1, f32[2]{0:T(128)} %refs_1_.1, s32[2,8]{1,0:T(2,128)} %bitcast.18, bf16[8,1024]{1,0:T(8,128)(2,1)} %refs_3_.1, bf16[1024,128]{1,0:T(8,128)(2,1)} %refs_4_.1, bf16[8,1,1024,128]{3,2,1,0:T(8,128)(2,1)} %refs_5_.1, ...), custom_call_target="tpu_custom_call" | custom-call | tf_op jit(solution)/shard_map/pallas_call | solution.py:641
  30.1 1.3 %shard_map.204 = (bf16[8,256]{1,0:T(8,128)(2,1)}, bf16[8,128]{1,0:T(8,128)(2,1)}) custom-call(bf16[8,256]{1,0:T(8,128)(2,1)} %get-tuple-element.6.result_ref, bf16[8,128]{1,0:T(8,128)(2,1)} %get-tuple-element.7.new_kv_ref), custom_call_target="tpu_custom_call" | custom-call | tf_op jit(solution)/shard_map/pallas_call | solution.py:657
